TPU v7x, 32 devices: a whole 2x2x4 slice. The times are simulated.
32 devices in a mesh: ep: 8 (over z, core), tp: 4 (over y, x).
Axes of the slice: x: 2, y: 2, z: 4, core: 2. Of those that a mesh axis runs over, the one named last changes fastest.
Arguments:
- tokens: bfloat16 [1024, 4096], P('ep', 'tp'), may hold values from -6 to 6
- out_grad: bfloat16 [1024, 4096], P('ep', 'tp'), may hold values from -1.5 to 1.5
- routes: int32 [1024, 2], P('ep'), may hold values from 0 to 7, all different within a row; in each aligned block of 128 rows (0 to 127, 128 to 255, ...) at most 40 rows name the same one
- route_weights: float32 [1024, 2], P('ep'), may hold values from 0.2 to 1.2
- gate_proj: bfloat16 [8, 1024, 4096], P('ep', 'tp'), may hold values from -0.09375 to 0.09375
- up_proj: bfloat16 [8, 1024, 4096], P('ep', 'tp'), may hold values from -0.09375 to 0.09375
- down_proj: bfloat16 [8, 1024, 4096], P('ep', 'tp'), may hold values from -0.1875 to 0.1875
- shared_hidden: bfloat16 [1024, 1024], P('ep'), may hold values from -6 to 6
Outputs:
- token_grad: bfloat16 [1024, 4096], P('ep', 'tp')
- weight_grad: float32 [1024, 2], P('ep')
- gate_grad: bfloat16 [8, 1024, 4096], P('ep', 'tp')
- up_grad: bfloat16 [8, 1024, 4096], P('ep', 'tp')
- down_grad: bfloat16 [8, 1024, 4096], P('ep', 'tp')
- shared_grad: float32 [1024, 4096], P('ep', 'tp')
Inputs may be any that keep to these rules, and one draw needn't show every extreme that they name: Within each block of 128 consecutive tokens, no expert is named by more than 40 routes, and in some blocks one expert is named by exactly 40. The 2 experts of one token differ.
All inputs are finite; a program needn't handle non-finite values.
Results may differ from a plain program's by a relative error of at most 0.0065.
Values may be sent and summed in bfloat16 or wider, within the bound.
A program may use at most 64 MiB of HBM per device.

v0:
```python
import jax
import jax.numpy as jnp
from jax import lax
from jax.sharding import PartitionSpec as P


def slot_tables(routes, num_experts, capacity):
    tok_rows, per_token = routes.shape
    route_count = tok_rows * per_token
    flat_routes = routes.reshape(-1)
    expert_ids = lax.broadcasted_iota(jnp.int32, (route_count, num_experts), 1)
    onehot = (flat_routes[:, None] == expert_ids).astype(jnp.int32)
    slot_rank = jnp.sum((jnp.cumsum(onehot, axis=0) - 1) * onehot, axis=1)
    slot_of_route = flat_routes * capacity + slot_rank
    slot_ids = lax.broadcasted_iota(jnp.int32, (num_experts * capacity, route_count), 0)
    route_ids = lax.broadcasted_iota(jnp.int32, (num_experts * capacity, route_count), 1)
    matches = slot_ids == slot_of_route[None, :]
    route_of_slot = jnp.sum(jnp.where(matches, route_ids, 0), axis=1)
    filled = jnp.any(matches, axis=1)
    return (slot_of_route, route_of_slot, filled)


def local(tokens, out_grad, routes, route_weights, gate_proj, up_proj, down_proj, shared_hidden):
    ep_count = lax.axis_size("ep")
    tp_count = lax.axis_size("tp")
    local_experts = gate_proj.shape[0]
    num_experts = local_experts * ep_count
    tok_rows, per_token = routes.shape
    capacity = max(2, 5 * tok_rows * per_token // (4 * num_experts))
    slot_of_route, route_of_slot, filled = slot_tables(routes, num_experts, capacity)
    token_of_slot = route_of_slot // per_token
    zero_value = jnp.zeros((), jnp.bfloat16)
    slot_weight = jnp.where(filled, route_weights.reshape(-1)[route_of_slot], 0.0)
    slot_weight = slot_weight.astype(jnp.bfloat16).reshape(ep_count, local_experts, capacity)
    layout = (ep_count, local_experts, capacity, -1)
    sent_tokens = jnp.where(filled[:, None], tokens[token_of_slot], zero_value).reshape(layout)
    sent_grads = jnp.where(filled[:, None], out_grad[token_of_slot], zero_value).reshape(layout)
    part_tokens, part_grads, weights_in = (
        lax.all_to_all(sent_tokens, "ep", split_axis=0, concat_axis=2, tiled=True),
        lax.all_to_all(sent_grads, "ep", split_axis=0, concat_axis=2, tiled=True),
        lax.all_to_all(slot_weight, "ep", split_axis=0, concat_axis=2, tiled=True),
    )
    rows_in, grads_in = (
        lax.all_gather(part_tokens, "tp", axis=3, tiled=True),
        lax.all_gather(part_grads, "tp", axis=3, tiled=True),
    )
    rows_in = rows_in[0]
    grads_in = grads_in[0]
    slot_scale = weights_in[0].astype(jnp.float32)
    pre_gate = jnp.einsum("lrd,lfd->lrf", rows_in, gate_proj, preferred_element_type=jnp.float32)
    pre_up = jnp.einsum("lrd,lfd->lrf", rows_in, up_proj, preferred_element_type=jnp.float32)
    squash = jax.nn.sigmoid(pre_gate)
    activated = pre_gate * squash
    hidden = (activated * pre_up).astype(jnp.bfloat16)
    back_grad = jnp.einsum("lrd,lfd->lrf", grads_in, down_proj, preferred_element_type=jnp.float32)
    partial_products = jnp.sum(hidden.astype(jnp.float32) * back_grad, axis=2)
    hidden_grad = slot_scale[:, :, None] * back_grad
    scaled_hidden = (slot_scale[:, :, None] * hidden.astype(jnp.float32)).astype(jnp.bfloat16)
    gate_delta = (hidden_grad * pre_up * squash * (1.0 + pre_gate * (1.0 - squash))).astype(
        jnp.bfloat16
    )
    up_delta = (hidden_grad * activated).astype(jnp.bfloat16)
    gate_grad = jnp.einsum(
        "lrf,lrd->lfd", gate_delta, rows_in, preferred_element_type=jnp.float32
    ).astype(jnp.bfloat16)
    up_grad = jnp.einsum(
        "lrf,lrd->lfd", up_delta, rows_in, preferred_element_type=jnp.float32
    ).astype(jnp.bfloat16)
    down_grad = jnp.einsum(
        "lrf,lrd->lfd", scaled_hidden, grads_in, preferred_element_type=jnp.float32
    ).astype(jnp.bfloat16)
    partial_rows = jnp.einsum(
        "lrf,lfd->lrd", gate_delta, gate_proj, preferred_element_type=jnp.float32
    )
    partial_rows = partial_rows + jnp.einsum(
        "lrf,lfd->lrd", up_delta, up_proj, preferred_element_type=jnp.float32
    )
    partial_rows = partial_rows.astype(jnp.bfloat16)
    gathered = lax.all_to_all(partial_rows, "tp", split_axis=2, concat_axis=0, tiled=True)
    gathered = gathered.reshape((tp_count,) + partial_rows.shape[:2] + (-1,))
    summed = jnp.sum(gathered, axis=0, dtype=jnp.float32)
    products = lax.psum(partial_products, "tp")
    slot_rows, slot_products = (
        lax.all_to_all(summed[None], "ep", split_axis=2, concat_axis=0, tiled=True),
        lax.all_to_all(products[None], "ep", split_axis=2, concat_axis=0, tiled=True),
    )
    feature_width = slot_rows.shape[-1]
    slot_rows = slot_rows.reshape(num_experts * capacity, feature_width)
    route_rows = slot_rows[slot_of_route].reshape(tok_rows, per_token, feature_width)
    token_grad = jnp.sum(route_rows, axis=1).astype(jnp.bfloat16)
    weight_grad = slot_products.reshape(-1)[slot_of_route].reshape(tok_rows, per_token)
    shared_grad = lax.psum_scatter(
        lax.dot_general(
            shared_hidden, out_grad, (((0,), (0,)), ((), ())), preferred_element_type=jnp.float32
        ),
        "ep",
        scatter_dimension=0,
        tiled=True,
    )
    return (token_grad, weight_grad, gate_grad, up_grad, down_grad, shared_grad)


def solution(mesh):
    return jax.shard_map(
        local,
        mesh=mesh,
        in_specs=(
            P("ep", "tp"),
            P("ep", "tp"),
            P("ep", None),
            P("ep", None),
            P("ep", "tp", None),
            P("ep", "tp", None),
            P("ep", "tp", None),
            P("ep", None),
        ),
        out_specs=(
            P("ep", "tp"),
            P("ep", None),
            P("ep", "tp", None),
            P("ep", "tp", None),
            P("ep", "tp", None),
            P("ep", "tp"),
        ),
        check_vma=False,
    )
```

profile of v0, /device:TPU:0, one launch (start us, length us, event | category | flops | bytes accessed | tf_op | source)
XLA Modules:
  0.0 350.5 jit_solution(12991959504227618092)
XLA Ops:
  8.1 1.0 copy.50
  9.3 0.6 reduce-window.6
  9.9 0.2 slice_reduce_fusion
  10.3 0.2 select_reduce_fusion
  10.4 0.2 fusion.23
  10.6 2.6 gather_fusion.1
  13.3 2.6 gather_fusion.2
  16.0 1.4 broadcast_select_fusion.1
  17.5 24.5 %all_to_all.60 = bf16[8,1,40,1024]{3,2,1,0:T(8,128)(2,1)} all-to-all(bf16[8,1,40,1024]{3,2,1,0:T(8,128)(2,1)S(1)} %get-tuple-element.43), channel_id=1, replica_groups=mesh['ep'=8,'tp'=4] {'ep'}, dimensions={0} | all-to-all | bytes 1310720 | tf_op jit(solution)/shard_map/all_to_all | solution.py:39
  42.1 21.2 %all_to_all.61 = bf16[8,1,40,1024]{3,2,1,0:T(8,128)(2,1)} all-to-all(bf16[8,1,40,1024]{3,2,1,0:T(8,128)(2,1)S(1)} %get-tuple-element.42), channel_id=1, replica_groups=mesh['ep'=8,'tp'=4] {'ep'}, dimensions={0} | all-to-all | bytes 1310720 | tf_op jit(solution)/shard_map/all_to_all | solution.py:40
  63.4 2.8 fusion.30
  66.2 0.7 copy-done.10
  67.1 2.4 gather_fusion
  69.6 8.1 %all_to_all.62 = bf16[8,1,40]{2,1,0:T(2,128)(2,1)S(1)} all-to-all(bf16[8,1,40]{2,1,0:T(2,128)(2,1)S(1)} %convert_element_type.110), channel_id=1, replica_groups=mesh['ep'=8,'tp'=4] {'ep'}, dimensions={0} | all-to-all | bytes 1280 | tf_op jit(solution)/shard_map/all_to_all | solution.py:41
  77.8 2.8 all-gather.5.cloned.1.call-done
  80.6 2.8 fusion.7
  83.4 0.4 copy-done.6
  83.9 0.9 fusion.9
  84.8 37.3 %all-gather.3.cloned.1.call-done = bf16[1,1,320,4096]{3,2,1,0:T(8,128)(2,1)} async-done(((bf16[1,1,320,1024]{3,2,1,0:T(8,128)(2,1)}), bf16[1,1,320,4096]{3,2,1,0:T(8,128)(2,1)}) %all-gather.3.cloned.1.call-update) | async-done | bytes 2621456 | tf_op jit(solution)/shard_map/all_gather | solution.py:45
  122.0 3.4 fusion.20
  125.4 0.8 fusion.14
  126.3 0.7 copy-done.7
  127.0 2.4 fusion.1
  129.4 14.3 %copy.56 = bf16[1,320,4096]{1,0,2:T(2,128)(2,1)} copy(bf16[1,320,4096]{2,1,0:T(8,128)(2,1)} %fusion.1) | data formatting | bytes 5242880 | tf_op jit(solution)/shard_map/convert_element_type | solution.py:78
  143.7 0.5 broadcast.230
  144.3 68.8 %reduce.16 = bf16[4096,320]{1,0:T(8,128)(2,1)} reduce(bf16[4096,1,320]{2,1,0:T(2,128)(2,1)} %bitcast.67, bf16[]{:T(256)} %broadcast.230), dimensions={1}, to_apply=%bitcast.53.reduce_sub_computation | reduce | bytes 5242882
  213.0 6.1 %reshape.388 = bf16[4,2,163840]{2,1,0:T(2,128)(2,1)} reshape(bf16[4096,320]{1,0:T(8,128)(2,1)} %reduce.16) | data formatting | bytes 5242880
  219.2 4.6 %all-to-all-start.3 = ((bf16[4,2,163840]{2,1,0:T(2,128)(2,1)}), bf16[4,2,163840]{2,1,0:T(2,128)(2,1)}, u32[]{:S(2)}, u32[]{:S(2)}) async-start(bf16[4,2,163840]{2,1,0:T(2,128)(2,1)} %reshape.388), calls=%async_computation.3 | async-start | bytes 5242880 | tf_op jit(solution)/shard_map/all_to_all | solution.py:79
  223.8 33.7 %psum.7 = f32[1,1,320]{2,1,0:T(1,128)S(1)} all-reduce(f32[1,1,320]{2,1,0:T(1,128)S(1)} %broadcast_in_dim.48), channel_id=1, replica_groups=mesh['ep'=8,'tp'=4] {'tp'}, use_global_device_ids=true, to_apply=%region_8.9 | all-reduce | flops 320 | bytes 2560 | tf_op jit(solution)/shard_map/psum | solution.py:82
  257.5 0.8 copy.59
  258.3 4.6 %all-to-all-start.5 = ((f32[1,1,320]{1,0,2:T(1,128)}), f32[1,1,320]{1,0,2:T(1,128)S(1)}, u32[]{:S(2)}, u32[]{:S(2)}) async-start(f32[1,1,320]{1,0,2:T(1,128)} %copy.59), calls=%async_computation.5 | async-start | bytes 327680 | tf_op jit(solution)/shard_map/all_to_all | solution.py:85
  262.9 7.6 %reshape.389 = bf16[4096,1,320]{2,1,0:T(2,128)(2,1)} reshape(bf16[4,2,163840]{2,1,0:T(2,128)(2,1)} %all-to-all-done.3) | data formatting | bytes 5242880
  270.5 14.0 %copy.57 = bf16[1,320,4096]{2,1,0:T(8,128)(2,1)} copy(bf16[1,320,4096]{1,0,2:T(2,128)(2,1)} %bitcast.68) | data formatting | bytes 5242880 | tf_op jit(solution)/shard_map/all_to_all | solution.py:79
  284.5 7.3 %reshape.336 = f32[320,4,1024]{2,1,0:T(4,128)} reshape(bf16[1,320,4096]{2,1,0:T(8,128)(2,1)} %copy.57) | data formatting | bytes 7864320 | tf_op jit(solution)/shard_map/convert_element_type | solution.py:81
  291.8 5.7 %reduce_sum.54 = f32[320,1024]{1,0:T(8,128)S(1)} reduce(f32[320,4,1024]{2,1,0:T(4,128)} %reshape.336, f32[]{:T(128)} %constant.33.clone.1), dimensions={1}, to_apply=%region_5.6 | reduce | flops 983040 | bytes 6553604 | tf_op jit(solution)/shard_map/reduce_sum | solution.py:81
  297.5 2.0 broadcast_in_dim.47
  299.5 5.1 %all-to-all-start.4 = ((f32[1,1,320,1024]{3,1,0,2:T(1,128)}), f32[1,1,320,1024]{3,1,0,2:T(1,128)S(1)}, u32[]{:S(2)}, u32[]{:S(2)}) async-start(f32[1,1,320,1024]{3,1,0,2:T(1,128)} %broadcast_in_dim.47), calls=%async_computation.4 | async-start | bytes 2621440 | tf_op jit(solution)/shard_map/all_to_all | solution.py:84
  304.9 4.3 %fusion.2 = bf16[1,256,4096]{2,1,0:T(8,128)(2,1)} fusion(bf16[320,256]{1,0:T(8,128)(2,1)S(1)} %get-tuple-element.40, bf16[1,1,320,4096]{3,2,1,0:T(8,128)(2,1)} %all-gather.5.cloned.1.call-done), kind=kOutput, calls=%fused_computation.11 | convolution fusion | flops 672137216 | bytes 4882432 | tf_op jit(solution)/shard_map/lrf,lrd->lfd/dot_general | solution.py:63
  309.3 4.5 %fusion.3 = bf16[1,256,4096]{2,1,0:T(8,128)(2,1)} fusion(bf16[320,256]{1,0:T(8,128)(2,1)S(1)} %get-tuple-element.41, bf16[1,1,320,4096]{3,2,1,0:T(8,128)(2,1)} %all-gather.5.cloned.1.call-done), kind=kOutput, calls=%fused_computation.12 | convolution fusion | flops 672137216 | bytes 4882432 | tf_op jit(solution)/shard_map/lrf,lrd->lfd/dot_general | solution.py:66
  313.7 2.7 fusion.4
  316.4 1.1 reduce.9
  317.5 1.9 gather_fusion.4
  319.6 0.6 copy.60
  320.2 16.6 %all-to-all-done.4 = f32[1,1,320,1024]{3,1,0,2:T(1,128)S(1)} async-done(((f32[1,1,320,1024]{3,1,0,2:T(1,128)}), f32[1,1,320,1024]{3,1,0,2:T(1,128)S(1)}, u32[]{:S(2)}, u32[]{:S(2)}) %all-to-all-start.4) | async-done | bytes 1310752 | tf_op jit(solution)/shard_map/all_to_all | solution.py:84
  336.8 0.3 copy.63
  337.1 2.0 gather_fusion.3
  339.1 1.8 reshape.331
  341.0 2.1 reduce_sum.56
  (51 shorter events, 1.6 us)
Async XLA Ops:
  8.0 72.6 %copy-start = (bf16[1,256,4096]{2,1,0:T(8,128)(2,1)S(1)}, bf16[1,256,4096]{2,1,0:T(8,128)(2,1)}, u32[]{:S(2)}) copy-start(bf16[1,256,4096]{2,1,0:T(8,128)(2,1)} %param.12) | copy-start | bytes 6291460
  8.0 2.6 copy-start.2
  8.0 72.6 %all-gather.5.cloned.1.call-start = ((), (), s32[]{:S(2)}) async-start(), calls=%async_computation.8 | async-start | bytes 3276800 | tf_op jit(solution)/shard_map/all_gather | solution.py:44
  10.6 2.7 copy-start.3
  17.5 45.9 %copy-start.8 = (bf16[128,1024]{1,0:T(8,128)(2,1)S(1)}, bf16[128,1024]{1,0:T(8,128)(2,1)}, u32[]{:S(2)}) copy-start(bf16[128,1024]{1,0:T(8,128)(2,1)} %param.15) | copy-start | bytes 786436
  42.0 80.0 %all-gather.3.cloned.1.call-start = ((), (), s32[]{:S(2)}) async-start(), calls=%async_computation.7 | async-start | bytes 3276800 | tf_op jit(solution)/shard_map/all_gather | solution.py:45
  63.3 279.7 %reduce-scatter.2.cloned.1.call-start = ((), (), s32[]{:S(2)}) async-start(), calls=%async_computation.9 | async-start | bytes 4718592 | tf_op jit(solution)/shard_map/reduce_scatter | solution.py:92
  66.2 0.7 copy-start.10
  80.6 2.8 copy-start.4
  80.6 3.2 copy-start.6
  125.4 1.6 copy-start.7
  219.2 39.1 %all-to-all-start.3 = ((bf16[4,2,163840]{2,1,0:T(2,128)(2,1)}), bf16[4,2,163840]{2,1,0:T(2,128)(2,1)}, u32[]{:S(2)}, u32[]{:S(2)}) async-start(bf16[4,2,163840]{2,1,0:T(2,128)(2,1)} %reshape.388), calls=%async_computation.3 | async-start | bytes 5242880 | tf_op jit(solution)/shard_map/all_to_all | solution.py:79
  258.3 41.2 %all-to-all-start.5 = ((f32[1,1,320]{1,0,2:T(1,128)}), f32[1,1,320]{1,0,2:T(1,128)S(1)}, u32[]{:S(2)}, u32[]{:S(2)}) async-start(f32[1,1,320]{1,0,2:T(1,128)} %copy.59), calls=%async_computation.5 | async-start | bytes 327680 | tf_op jit(solution)/shard_map/all_to_all | solution.py:85
  297.5 7.1 %copy-start.9 = (s32[128,2]{0,1:T(2,128)S(1)}, s32[128,2]{0,1:T(2,128)}, u32[]{:S(2)}) copy-start(s32[128,2]{0,1:T(2,128)} %param.10) | copy-start | bytes 3076
  299.5 37.3 %all-to-all-start.4 = ((f32[1,1,320,1024]{3,1,0,2:T(1,128)}), f32[1,1,320,1024]{3,1,0,2:T(1,128)S(1)}, u32[]{:S(2)}, u32[]{:S(2)}) async-start(f32[1,1,320,1024]{3,1,0,2:T(1,128)} %broadcast_in_dim.47), calls=%async_computation.4 | async-start | bytes 2621440 | tf_op jit(solution)/shard_map/all_to_all | solution.py:84
  309.3 4.5 %copy-start.5 = (bf16[1,1,320,4096]{3,2,1,0:T(8,128)(2,1)S(1)}, bf16[1,1,320,4096]{3,2,1,0:T(8,128)(2,1)}, u32[]{:S(2)}) copy-start(bf16[1,1,320,4096]{3,2,1,0:T(8,128)(2,1)} %all-gather.3.cloned.1.call-done) | copy-start | bytes 7864324
  337.1 6.0 %copy-start.1 = (bf16[1,256,4096]{2,1,0:T(8,128)(2,1)S(1)}, bf16[1,256,4096]{2,1,0:T(8,128)(2,1)}, u32[]{:S(2)}) copy-start(bf16[1,256,4096]{2,1,0:T(8,128)(2,1)} %param.12) | copy-start | bytes 6291460
Sparse Core Ops, SparseCore 0:
  42.1 38.4 all-gather.4
  82.5 39.4 all-gather.2
Sparse Core Ops, SparseCore 1:
  66.7 48.8 reduce-scatter.1
where the time goes:
time: 352 us; the launch traced here: 350 us
  blocking collectives  87.6 us (25%)
  other arithmetic  80.1 us (23%)
  local copies, waits for them, and re-layouts  71.3 us (20%)
  waiting for transfers between devices  56.7 us (16%)
  matrix products  24.6 us (7%)
  between operations  15.7 us (4%)
  starting transfers between devices  14.4 us (4%)
    unnamed x1, other arithmetic  68.8 us
    all_gather x1, waiting for transfers between devices, local(): lax.all_gather(part_grads, 'tp', axis=3, tiled=True)  37.3 us
    psum x1, blocking collectives, local(): products = lax.psum(partial_products, 'tp')  33.7 us
    all_to_all x1, blocking collectives, local(): lax.all_to_all(sent_tokens, 'ep', split_axis=0, concat_axis=2, tiled=True)  24.5 us
    all_to_all x1, blocking collectives, local(): lax.all_to_all(sent_grads, 'ep', split_axis=0, concat_axis=2, tiled=True)  21.2 us
    unnamed x29, local copies, waits for them, and re-layouts  18.1 us
    all_to_all x1, waiting for transfers between devices, local(): lax.all_to_all(summed[None], 'ep', split_axis=2, concat_axis=0, tiled=True)  16.6 us
    convert_element_type x1, local copies, waits for them, and re-layouts, local(): partial_rows = partial_rows.astype(jnp.bfloat16)  14.3 us
  transfers between devices with their start and end apart: 6, of which 3 were waited for; matrix products, arithmetic and copies ran while one was open for 47% of the time, Pallas kernels for 0%

commit v1 on v0

--- a/solution.py
+++ b/solution.py
@@ -76,7 +76,10 @@
         "lrf,lfd->lrd", up_delta, up_proj, preferred_element_type=jnp.float32
     )
     partial_rows = partial_rows.astype(jnp.bfloat16)
-    gathered = lax.all_to_all(partial_rows, "tp", split_axis=2, concat_axis=0, tiled=True)
+    gathered = jnp.concatenate(
+        lax.all_to_all(jnp.stack(jnp.split(partial_rows, lax.axis_size("tp"), axis=2)), "tp", 0, 0),
+        axis=0,
+    )
     gathered = gathered.reshape((tp_count,) + partial_rows.shape[:2] + (-1,))
     summed = jnp.sum(gathered, axis=0, dtype=jnp.float32)
     products = lax.psum(partial_products, "tp")

time: 352 us -> 233 us (0.66)
  other arithmetic: 80.1 us -> 9.95 us
  local copies, waits for them, and re-layouts: 71.3 us -> 22.9 us
  waiting for transfers between devices: 56.7 us -> 60.4 us
    unnamed x1 -> x0, other arithmetic: 68.8 us -> none
    convert_element_type x2 -> x0, local copies, waits for them, and re-layouts: 21.7 us -> none  [the longest x1 14.3 us: local(): partial_rows = partial_rows.astype(jnp.bfloat16)]
    all_to_all x1 -> x0, local copies, waits for them, and re-layouts: 14 us -> none  [local(): lax.all_to_all(partial_rows, 'tp', split_axis=2, concat_axis=0, tiled=True)]
    unnamed x29 -> x26, local copies, waits for them, and re-layouts: 18.1 us -> 5.17 us
  transfers between devices with their start and end apart: 6 -> 6, of which waited for: 3 -> 4; matrix products, arithmetic and copies ran while one was open for 47% -> 19% of each run, Pallas kernels for 0% -> 0%
where the time goes in v1:
time: 233 us; the launch traced here: 232 us
  blocking collectives  87.6 us (38%)
  waiting for transfers between devices  60.4 us (26%)
  local copies, waits for them, and re-layouts  22.9 us (10%)
  matrix products  22 us (9%)
  between operations  15.8 us (7%)
  starting transfers between devices  13.7 us (6%)
  other arithmetic  9.95 us (4%)
    all_gather x1, waiting for transfers between devices, local(): lax.all_gather(part_grads, 'tp', axis=3, tiled=True)  36.5 us
    psum x1, blocking collectives, local(): products = lax.psum(partial_products, 'tp')  33.7 us
    all_to_all x1, blocking collectives, local(): lax.all_to_all(sent_tokens, 'ep', split_axis=0, concat_axis=2, tiled=True)  24.5 us
    all_to_all x1, blocking collectives, local(): lax.all_to_all(sent_grads, 'ep', split_axis=0, concat_axis=2, tiled=True)  21.2 us
    all_to_all x1, waiting for transfers between devices, local(): lax.all_to_all(summed[None], 'ep', split_axis=2, concat_axis=0, tiled=True)  18.1 us
    all_to_all x1, blocking collectives, local(): lax.all_to_all(slot_weight, 'ep', split_axis=0, concat_axis=2, tiled=True)  8.11 us
    unnamed x26, local copies, waits for them, and re-layouts  5.17 us
  transfers between devices with their start and end apart: 6, of which 4 were waited for; matrix products, arithmetic and copies ran while one was open for 19% of the time, Pallas kernels for 0%

profile of v1, /device:TPU:0, one launch (start us, length us, event | category | flops | bytes accessed | tf_op | source)
XLA Modules:
  0.0 232.3 jit_solution(4868242754059209188)
XLA Ops:
  8.1 1.0 copy.36
  9.0 0.1 eq.26
  9.2 0.1 reshape.315
  9.3 0.6 reduce-window.6
  9.9 0.2 slice_reduce_fusion
  10.3 0.2 select_reduce_fusion
  10.4 0.2 fusion.23
  10.6 2.6 %gather_fusion.1 = bf16[320,1024]{1,0:T(8,128)(2,1)} fusion(bf16[128,1024]{1,0:T(8,128)(2,1)S(1)} %copy-done.1, s32[1024]{0:T(1024)S(1)} %get-tuple-element.42), kind=kCustom, calls=%fused_computation.1 | custom fusion | bytes 1312000 | tf_op jit(solution)/shard_map/gather | solution.py:37
  13.3 2.6 %gather_fusion.2 = bf16[320,1024]{1,0:T(8,128)(2,1)} fusion(bf16[128,1024]{1,0:T(8,128)(2,1)S(1)} %copy-done.2, s32[1024]{0:T(1024)S(1)} %get-tuple-element.42), kind=kCustom, calls=%fused_computation.2 | custom fusion | bytes 1312000 | tf_op jit(solution)/shard_map/gather | solution.py:36
  16.0 1.4 broadcast_select_fusion.1
  17.5 24.5 %all_to_all.56 = bf16[8,1,40,1024]{3,2,1,0:T(8,128)(2,1)} all-to-all(bf16[8,1,40,1024]{3,2,1,0:T(8,128)(2,1)S(1)} %get-tuple-element.41), channel_id=1, replica_groups=mesh['ep'=8,'tp'=4] {'ep'}, dimensions={0} | all-to-all | bytes 1310720 | tf_op jit(solution)/shard_map/all_to_all | solution.py:39
  42.1 21.2 %all_to_all.57 = bf16[8,1,40,1024]{3,2,1,0:T(8,128)(2,1)} all-to-all(bf16[8,1,40,1024]{3,2,1,0:T(8,128)(2,1)S(1)} %get-tuple-element.40), channel_id=1, replica_groups=mesh['ep'=8,'tp'=4] {'ep'}, dimensions={0} | all-to-all | bytes 1310720 | tf_op jit(solution)/shard_map/all_to_all | solution.py:40
  63.4 2.7 %fusion.30 = f32[1024,1024]{1,0:T(8,128)} fusion(bf16[128,1024]{1,0:T(8,128)(2,1)S(1)} %copy-done.8, bf16[128,1024]{1,0:T(8,128)(2,1)S(1)} %copy-done.1), kind=kOutput, calls=%fused_computation.73 | convolution fusion | flops 268435456 | bytes 4718592 | tf_op jit(solution)/shard_map/dot_general | solution.py:96
  66.1 0.7 copy-done.10
  66.9 0.1 reshape.317
  67.0 2.4 %gather_fusion = bf16[320]{0:T(512)(128)(2,1)S(1)} fusion(bf16[256]{0:T(256)(128)(2,1)S(1)} %reshape.317, s32[1024]{0:T(1024)S(1)} %get-tuple-element.43), kind=kCustom, calls=%fused_computation | custom fusion | bytes 2560 | tf_op jit(solution)/shard_map/gather | solution.py:33
  69.5 8.1 %all_to_all.58 = bf16[8,1,40]{2,1,0:T(2,128)(2,1)S(1)} all-to-all(bf16[8,1,40]{2,1,0:T(2,128)(2,1)S(1)} %convert_element_type.102), channel_id=1, replica_groups=mesh['ep'=8,'tp'=4] {'ep'}, dimensions={0} | all-to-all | bytes 1280 | tf_op jit(solution)/shard_map/all_to_all | solution.py:41
  77.7 2.9 %all-gather.5.cloned.1.call-done = bf16[1,1,320,4096]{3,2,1,0:T(8,128)(2,1)} async-done(((bf16[1,1,320,1024]{3,2,1,0:T(8,128)(2,1)}), bf16[1,1,320,4096]{3,2,1,0:T(8,128)(2,1)}) %all-gather.5.cloned.1.call-update) | async-done | bytes 2621456 | tf_op jit(solution)/shard_map/all_gather | solution.py:44
  80.6 2.8 %fusion.7 = f32[320,256]{1,0:T(8,128)S(1)} fusion(bf16[1,1,320,4096]{3,2,1,0:T(8,128)(2,1)} %all-gather.5.cloned.1.call-done, bf16[1,256,4096]{2,1,0:T(8,128)(2,1)S(1)} %copy-done), kind=kOutput, calls=%fused_computation.18 | convolution fusion | flops 671088640 | bytes 5046272 | tf_op jit(solution)/shard_map/lrd,lfd->lrf/dot_general | solution.py:50
  83.4 0.4 copy-done.6
  83.9 1.6 fusion.9
  85.5 36.5 %all-gather.3.cloned.1.call-done = bf16[1,1,320,4096]{3,2,1,0:T(8,128)(2,1)} async-done(((bf16[1,1,320,1024]{3,2,1,0:T(8,128)(2,1)}), bf16[1,1,320,4096]{3,2,1,0:T(8,128)(2,1)}) %all-gather.3.cloned.1.call-update) | async-done | bytes 2621456 | tf_op jit(solution)/shard_map/all_gather | solution.py:45
  122.0 3.4 %fusion.20 = (f32[320]{0:T(512)S(1)}, bf16[320,256]{1,0:T(8,128)(2,1)S(1)}, bf16[320,256]{1,0:T(8,128)(2,1)S(1)}, bf16[320,256]{1,0:T(8,128)(2,1)S(1)}) fusion(f32[320,256]{1,0:T(8,128)} %fusion.9, f32[320,256]{1,0:T(8,128)S(1)} %fusion.7, f32[320]{0:T(512)S(1)} %reshape.328, bf16[1,256,4096]{2,1,0:T(8,128)(2,1)} %param.14, ...), kind=kOutput, calls=%fused_computation.40 | convolution fusion | flops 672644800 | bytes 5868032 | tf_op jit(solution)/shard_map/lrd,lfd->lrf/dot_general | solution.py:55
  125.4 0.8 fusion.14
  126.3 0.7 copy-done.7
  127.0 0.9 fusion.1
  127.9 0.3 slice_bitcast_fusion.3
  128.2 1.9 pad_maximum_fusion
  130.0 4.5 %all-to-all-start.3 = ((bf16[4,1,320,1024]{3,2,1,0:T(8,128)(2,1)}), bf16[4,1,320,1024]{3,2,1,0:T(8,128)(2,1)}, u32[]{:S(2)}, u32[]{:S(2)}) async-start(bf16[4,1,320,1024]{3,2,1,0:T(8,128)(2,1)} %pad_maximum_fusion), calls=%async_computation.3 | async-start | bytes 5242880 | tf_op jit(solution)/shard_map/all_to_all | solution.py:80
  134.6 33.7 %psum.7 = f32[1,1,320]{2,1,0:T(1,128)S(1)} all-reduce(f32[1,1,320]{2,1,0:T(1,128)S(1)} %broadcast_in_dim.48), channel_id=1, replica_groups=mesh['ep'=8,'tp'=4] {'tp'}, use_global_device_ids=true, to_apply=%region_8.9 | all-reduce | flops 320 | bytes 2560 | tf_op jit(solution)/shard_map/psum | solution.py:85
  168.3 0.8 copy.43
  169.1 4.6 %all-to-all-start.5 = ((f32[1,1,320]{1,0,2:T(1,128)}), f32[1,1,320]{1,0,2:T(1,128)S(1)}, u32[]{:S(2)}, u32[]{:S(2)}) async-start(f32[1,1,320]{1,0,2:T(1,128)} %copy.43), calls=%async_computation.5 | async-start | bytes 327680 | tf_op jit(solution)/shard_map/all_to_all | solution.py:88
  173.7 2.4 %convert_reduce_fusion = f32[320,1024]{1,0:T(8,128)S(1)} fusion(bf16[4,1,320,1024]{3,2,1,0:T(8,128)(2,1)} %all-to-all-done.3), kind=kLoop, calls=%fused_computation.7 | loop fusion | flops 2293760 | bytes 3932160 | tf_op jit(solution)/shard_map/reduce_sum | solution.py:84
  176.1 2.0 broadcast_in_dim.47
  178.1 2.8 %all-to-all-done.5 = f32[1,1,320]{1,0,2:T(1,128)S(1)} async-done(((f32[1,1,320]{1,0,2:T(1,128)}), f32[1,1,320]{1,0,2:T(1,128)S(1)}, u32[]{:S(2)}, u32[]{:S(2)}) %all-to-all-start.5) | async-done | bytes 1312 | tf_op jit(solution)/shard_map/all_to_all | solution.py:88
  180.9 4.5 %all-to-all-start.4 = ((f32[1,1,320,1024]{3,1,0,2:T(1,128)}), f32[1,1,320,1024]{3,1,0,2:T(1,128)}, u32[]{:S(2)}, u32[]{:S(2)}) async-start(f32[1,1,320,1024]{3,1,0,2:T(1,128)} %broadcast_in_dim.47), calls=%async_computation.4 | async-start | bytes 2621440 | tf_op jit(solution)/shard_map/all_to_all | solution.py:87
  185.5 0.1 mul.88
  185.7 4.5 %fusion.2 = bf16[1,256,4096]{2,1,0:T(8,128)(2,1)} fusion(bf16[320,256]{1,0:T(8,128)(2,1)S(1)} %get-tuple-element.38, bf16[1,1,320,4096]{3,2,1,0:T(8,128)(2,1)} %all-gather.5.cloned.1.call-done), kind=kOutput, calls=%fused_computation.12 | convolution fusion | flops 672137216 | bytes 4882432 | tf_op jit(solution)/shard_map/lrf,lrd->lfd/dot_general | solution.py:63
  190.2 2.6 %fusion.3 = bf16[1,256,4096]{2,1,0:T(8,128)(2,1)} fusion(bf16[320,256]{1,0:T(8,128)(2,1)S(1)} %get-tuple-element.39, bf16[1,1,320,4096]{3,2,1,0:T(8,128)(2,1)S(1)} %copy-done.4), kind=kOutput, calls=%fused_computation.13 | convolution fusion | flops 672137216 | bytes 4882432 | tf_op jit(solution)/shard_map/lrf,lrd->lfd/dot_general | solution.py:66
  192.8 2.7 %fusion.4 = bf16[1,256,4096]{2,1,0:T(8,128)(2,1)} fusion(bf16[1,1,320,4096]{3,2,1,0:T(8,128)(2,1)S(1)} %copy-done.5, bf16[320,256]{1,0:T(8,128)(2,1)S(1)} %get-tuple-element.33, f32[320]{0:T(512)S(1)} %reshape.328), kind=kOutput, calls=%fused_computation.14 | convolution fusion | flops 672382976 | bytes 4883712 | tf_op jit(solution)/shard_map/lrf,lrd->lfd/dot_general | solution.py:69
  195.5 1.1 reduce.7
  196.5 1.9 gather_fusion.4
  198.6 0.6 copy.44
  199.3 18.1 %all-to-all-done.4 = f32[1,1,320,1024]{3,1,0,2:T(1,128)} async-done(((f32[1,1,320,1024]{3,1,0,2:T(1,128)}), f32[1,1,320,1024]{3,1,0,2:T(1,128)}, u32[]{:S(2)}, u32[]{:S(2)}) %all-to-all-start.4) | async-done | bytes 1310752 | tf_op jit(solution)/shard_map/all_to_all | solution.py:87
  217.4 1.6 copy.47
  219.0 2.0 gather_fusion.3
  221.0 1.8 reshape.324
  222.8 2.1 reduce_sum.56
  (46 shorter events, 1.1 us)
Async XLA Ops:
  8.0 72.6 %copy-start = (bf16[1,256,4096]{2,1,0:T(8,128)(2,1)S(1)}, bf16[1,256,4096]{2,1,0:T(8,128)(2,1)}, u32[]{:S(2)}) copy-start(bf16[1,256,4096]{2,1,0:T(8,128)(2,1)} %param.12) | copy-start | bytes 6291460
  8.0 2.6 %copy-start.1 = (bf16[128,1024]{1,0:T(8,128)(2,1)S(1)}, bf16[128,1024]{1,0:T(8,128)(2,1)}, u32[]{:S(2)}) copy-start(bf16[128,1024]{1,0:T(8,128)(2,1)} %param.9) | copy-start | bytes 786436
  8.0 72.6 %all-gather.5.cloned.1.call-start = ((), (), s32[]{:S(2)}) async-start(), calls=%async_computation.8 | async-start | bytes 3276800 | tf_op jit(solution)/shard_map/all_gather | solution.py:44
  10.6 2.7 %copy-start.2 = (bf16[128,1024]{1,0:T(8,128)(2,1)S(1)}, bf16[128,1024]{1,0:T(8,128)(2,1)}, u32[]{:S(2)}) copy-start(bf16[128,1024]{1,0:T(8,128)(2,1)} %param.8) | copy-start | bytes 786436
  17.5 45.9 %copy-start.8 = (bf16[128,1024]{1,0:T(8,128)(2,1)S(1)}, bf16[128,1024]{1,0:T(8,128)(2,1)}, u32[]{:S(2)}) copy-start(bf16[128,1024]{1,0:T(8,128)(2,1)} %param.15) | copy-start | bytes 786436
  42.0 80.0 %all-gather.3.cloned.1.call-start = ((), (), s32[]{:S(2)}) async-start(), calls=%async_computation.7 | async-start | bytes 3276800 | tf_op jit(solution)/shard_map/all_gather | solution.py:45
  63.3 161.6 %reduce-scatter.2.cloned.1.call-start = ((), (), s32[]{:S(2)}) async-start(), calls=%async_computation.9 | async-start | bytes 4718592 | tf_op jit(solution)/shard_map/reduce_scatter | solution.py:95
  66.0 0.7 copy-start.10
  80.6 2.8 %copy-start.3 = (bf16[1,1,320,4096]{3,2,1,0:T(8,128)(2,1)S(1)}, bf16[1,1,320,4096]{3,2,1,0:T(8,128)(2,1)}, u32[]{:S(2)}) copy-start(bf16[1,1,320,4096]{3,2,1,0:T(8,128)(2,1)} %all-gather.5.cloned.1.call-done) | copy-start | bytes 7864324
  80.6 3.2 %copy-start.6 = (bf16[1,256,4096]{2,1,0:T(8,128)(2,1)S(1)}, bf16[1,256,4096]{2,1,0:T(8,128)(2,1)}, u32[]{:S(2)}) copy-start(bf16[1,256,4096]{2,1,0:T(8,128)(2,1)} %param.13) | copy-start | bytes 6291460
  125.4 1.6 copy-start.7
  130.0 39.1 %all-to-all-start.3 = ((bf16[4,1,320,1024]{3,2,1,0:T(8,128)(2,1)}), bf16[4,1,320,1024]{3,2,1,0:T(8,128)(2,1)}, u32[]{:S(2)}, u32[]{:S(2)}) async-start(bf16[4,1,320,1024]{3,2,1,0:T(8,128)(2,1)} %pad_maximum_fusion), calls=%async_computation.3 | async-start | bytes 5242880 | tf_op jit(solution)/shard_map/all_to_all | solution.py:80
  169.1 11.8 %all-to-all-start.5 = ((f32[1,1,320]{1,0,2:T(1,128)}), f32[1,1,320]{1,0,2:T(1,128)S(1)}, u32[]{:S(2)}, u32[]{:S(2)}) async-start(f32[1,1,320]{1,0,2:T(1,128)} %copy.43), calls=%async_computation.5 | async-start | bytes 327680 | tf_op jit(solution)/shard_map/all_to_all | solution.py:88
  176.1 9.2 %copy-start.9 = (s32[128,2]{0,1:T(2,128)S(1)}, s32[128,2]{0,1:T(2,128)}, u32[]{:S(2)}) copy-start(s32[128,2]{0,1:T(2,128)} %param.10) | copy-start | bytes 3076
  180.9 36.5 %all-to-all-start.4 = ((f32[1,1,320,1024]{3,1,0,2:T(1,128)}), f32[1,1,320,1024]{3,1,0,2:T(1,128)}, u32[]{:S(2)}, u32[]{:S(2)}) async-start(f32[1,1,320,1024]{3,1,0,2:T(1,128)} %broadcast_in_dim.47), calls=%async_computation.4 | async-start | bytes 2621440 | tf_op jit(solution)/shard_map/all_to_all | solution.py:87
  185.7 4.5 %copy-start.4 = (bf16[1,1,320,4096]{3,2,1,0:T(8,128)(2,1)S(1)}, bf16[1,1,320,4096]{3,2,1,0:T(8,128)(2,1)}, u32[]{:S(2)}) copy-start(bf16[1,1,320,4096]{3,2,1,0:T(8,128)(2,1)} %all-gather.5.cloned.1.call-done) | copy-start | bytes 7864324
  190.2 2.6 %copy-start.5 = (bf16[1,1,320,4096]{3,2,1,0:T(8,128)(2,1)S(1)}, bf16[1,1,320,4096]{3,2,1,0:T(8,128)(2,1)}, u32[]{:S(2)}) copy-start(bf16[1,1,320,4096]{3,2,1,0:T(8,128)(2,1)} %all-gather.3.cloned.1.call-done) | copy-start | bytes 7864324
Sparse Core Ops, SparseCore 0:
  42.1 38.4 all-gather.4
  82.5 39.4 all-gather.2
Sparse Core Ops, SparseCore 1:
  66.7 48.8 reduce-scatter.1
